TPU v7x, 32 devices: a whole 2x2x4 slice. The times are simulated.
32 devices in a mesh: sp: 4 (over y, x), dp: 8 (over z, core).
Axes of the slice: x: 2, y: 2, z: 4, core: 2. Of those that a mesh axis runs over, the one named last changes fastest.
Arguments:
- value_half: bfloat16 [8, 1024, 2048], P('dp', 'sp'), may hold values from -6 to 6
- gate_half: bfloat16 [8, 1024, 2048], P('dp', 'sp'), may hold values from -6 to 6
- upstream: bfloat16 [8, 1024, 2048], P('dp', 'sp'), may hold values from -6 to 6
- conv_taps: float32 [31, 2048], P(None, 'sp'), may hold values from -1 to 1
- norm_gain: float32 [2048], replicated, may hold values from 0.1 to 1.9
- out_weight: bfloat16 [2048, 2048], P('dp'), may hold values from -0.125 to 0.125
Outputs:
- grad_value: bfloat16 [8, 1024, 2048], P('dp', 'sp')
- grad_gate: bfloat16 [8, 1024, 2048], P('dp', 'sp')
- grad_taps: float32 [31, 2048], P(None, 'sp')
- grad_gain: float32 [2048], replicated
- grad_weight: float32 [2048, 2048], P('dp')
All inputs are finite; a program needn't handle non-finite values.
Results may differ from a plain program's by a relative error of at most 0.0062.
Values may be sent and summed in bfloat16 or wider, within the bound.
A program may use at most 128 MiB of HBM per device.

v0:
```python
import jax
import jax.numpy as jnp
from jax import lax
from jax.sharding import PartitionSpec as P

NORM_EPS = 1e-05


def body(value_half, gate_half, upstream, conv_taps, norm_gain, out_weight):
    f32 = jnp.float32
    tap_count = conv_taps.shape[0]
    halo = tap_count - 1
    sp = lax.axis_size("sp")
    onward = [(i, i + 1) for i in range(sp - 1)]
    back = [(i + 1, i) for i in range(sp - 1)]
    value = value_half[0].astype(f32)
    gate = gate_half[0].astype(f32)
    length = value.shape[0]
    weight = lax.all_gather(out_weight, "dp", axis=0, tiled=True)
    up = upstream[0]
    up_columns = lax.all_to_all(up, "dp", split_axis=1, concat_axis=0, tiled=True)
    taps = lax.all_gather(conv_taps, "sp", axis=1, tiled=True)
    tail = (value[length - halo :] * jax.nn.sigmoid(gate[length - halo :])).astype(jnp.bfloat16)
    before = lax.ppermute(tail, "sp", onward)
    sig_gate = jax.nn.sigmoid(gate)
    glu = (value * sig_gate).astype(jnp.bfloat16)
    padded = jnp.concatenate([before, glu], axis=0).astype(f32)
    conv = jnp.zeros((length, padded.shape[1]), f32)
    for j in range(tap_count):
        conv = conv + taps[j] * padded[j : j + length]
    conv = conv.astype(jnp.bfloat16).astype(f32)
    mean = jnp.mean(conv, axis=-1, keepdims=True)
    centered = conv - mean
    inv = lax.rsqrt(jnp.mean(centered * centered, axis=-1, keepdims=True) + NORM_EPS)
    normed = centered * inv
    scaled = normed * norm_gain
    sig = jax.nn.sigmoid(scaled)
    activated = (scaled * sig).astype(jnp.bfloat16)
    act_all = lax.all_gather(activated, "dp", axis=0, tiled=True)
    grad_act = jnp.dot(up, weight, preferred_element_type=f32)
    grad_scaled = grad_act * sig * (1.0 + scaled * (1.0 - sig))
    gain_part = jnp.sum(grad_scaled * normed, axis=0)
    g = grad_scaled * norm_gain
    grad_conv = inv * (
        g
        - jnp.mean(g, axis=-1, keepdims=True)
        - normed * jnp.mean(g * normed, axis=-1, keepdims=True)
    )
    grad_conv = grad_conv.astype(jnp.bfloat16)
    after = lax.ppermute(grad_conv[:halo], "sp", back)
    extended = jnp.concatenate([grad_conv, after], axis=0).astype(f32)
    here = grad_conv.astype(f32)
    grad_glu = jnp.zeros_like(here)
    terms = []
    for j in range(tap_count):
        first = halo - j
        grad_glu = grad_glu + taps[j] * extended[first : first + length]
        terms.append(jnp.sum(here * padded[j : j + length], axis=0))
    sums = lax.psum(jnp.stack(terms + [gain_part]), ("sp", "dp"))
    width = conv_taps.shape[1]
    grad_taps = lax.dynamic_slice_in_dim(
        sums[:tap_count], lax.axis_index("sp") * width, width, axis=1
    )
    grad_gain = sums[tap_count]
    grad_glu = grad_glu.astype(jnp.bfloat16).astype(f32)
    grad_value = (grad_glu * sig_gate).astype(jnp.bfloat16)
    grad_gate = (grad_glu * value * sig_gate * (1.0 - sig_gate)).astype(jnp.bfloat16)
    owned = lax.dot_general(
        up_columns, act_all, (((0,), (0,)), ((), ())), preferred_element_type=f32
    )
    grad_weight = lax.psum(owned, "sp")
    return (grad_value[None], grad_gate[None], grad_taps, grad_gain, grad_weight)


def solution(mesh):
    tokens = P("dp", "sp", None)
    return jax.shard_map(
        body,
        mesh=mesh,
        in_specs=(tokens, tokens, tokens, P(None, "sp"), P(), P("dp", None)),
        out_specs=(tokens, tokens, P(None, "sp"), P(), P("dp", None)),
        check_vma=False,
    )
```

profile of v0, /device:TPU:0, one launch (start us, length us, event | category | flops | bytes accessed | tf_op | source)
XLA Modules:
  0.0 418.7 jit_solution(15272837373244284159)
XLA Ops:
  7.2 0.0 all-gather.3.cloned.1.call-start
  7.2 0.7 all-gather.3.cloned.1.call-update
  7.9 0.0 all-gather.5.cloned.1.call-start
  8.0 1.5 convert_element_type.49
  9.5 0.2 convert_element_type.50
  9.7 0.1 fusion.96
  9.8 4.9 %collective-permute-start = (bf16[30,2048]{1,0:T(8,128)(2,1)S(1)}, bf16[30,2048]{1,0:T(8,128)(2,1)S(1)}, u32[]{:S(2)}, u32[]{:S(2)}) collective-permute-start(bf16[30,2048]{1,0:T(8,128)(2,1)S(1)} %fusion.96), channel_id=1, source_target_pairs={{0,8},{8,16},{16,24},{1,9},{9,17},{17,25},{2,10},{10,18},{18,26},{... | collective-permute-start | bytes 368648 | tf_op jit(solution)/shard_map/ppermute | solution.py:24
  14.7 9.1 %all_gather.9 = f32[31,2048]{1,0:T(8,128)S(1)} all-gather(f32[31,512]{1,0:T(8,128)S(1)} %copy-done.49), channel_id=1, replica_groups=mesh['sp'=4,'dp'=8] {'sp'}, dimensions={1}, use_global_device_ids=true | all-gather | bytes 317440 | tf_op jit(solution)/shard_map/all_gather | solution.py:22
  23.8 0.1 fusion.99
  24.1 0.6 fusion.87
  24.6 0.1 fusion.100
  24.8 0.3 maximum_convert_fusion
  25.3 10.7 %convert_reduce_fusion = (f32[256]{0:T(256)S(1)}, bf16[256,2048]{1,0:T(8,128)(2,1)S(1)}) fusion(f32[286,2048]{1,0:T(8,128)S(1)} %maximum_convert_fusion, f32[2048]{0:T(1024)S(1)} %bitcast.106, f32[2048]{0:T(1024)S(1)} %bitcast.108, f32[2048]{0:T(1024)S(1)} %bitcast.110, f32[2048]{0:T(1024)S(1)} %bitcast.112, f32[2048]{0:T(1024)S(1)} %bitcast.114, ...), kind=kLoop, calls=%fused_computation.37 | loop fusion | flops 33554176 | bytes 66315264 | tf_op jit(solution)/shard_map/reduce_sum | solution.py:32
  36.2 0.9 copy-done.3
  37.1 0.4 fusion.20
  37.6 56.8 %all-gather.3.cloned.1.call-done = bf16[2048,2048]{1,0:T(8,128)(2,1)} async-done(((bf16[256,2048]{1,0:T(8,128)(2,1)}), bf16[2048,2048]{1,0:T(8,128)(2,1)}) %all-gather.3.cloned.1.call-update) | async-done | bytes 8388624 | tf_op jit(solution)/shard_map/all_gather | solution.py:19
  94.4 9.5 %fusion.19 = (f32[2048]{0:T(1024)}, f32[256]{0:T(256)S(1)}, f32[256]{0:T(256)S(1)}, bf16[256,2048]{1,0:T(8,128)(2,1)}, f32[256,2048]{1,0:T(8,128)}) fusion(bf16[256,2048]{1,0:T(8,128)(2,1)} %copy-done.3, f32[256]{0:T(256)S(1)} %add_rsqrt_fusion, f32[256]{0:T(256)S(1)} %broadcast_multiply_fusion.2, f32[2048]{0:T(1024)} %param.10, ...), kind=kOutput, calls=%fused_computation.56 | convolution fusion | flops 2157966848 | bytes 13651968 | tf_op jit(solution)/shard_map/dot_general | solution.py:40
  103.9 0.0 all-gather.5.cloned.1.call-update
  103.9 2.3 copy.13
  106.2 4.4 %all-to-all-start = ((bf16[256,8,256]{0,2,1:T(8,128)(2,1)}), bf16[256,8,256]{0,2,1:T(8,128)(2,1)}, u32[]{:S(2)}, u32[]{:S(2)}) async-start(bf16[256,8,256]{0,2,1:T(8,128)(2,1)} %bitcast.102), calls=%async_computation | async-start | bytes 2097152 | tf_op jit(solution)/shard_map/all_to_all | solution.py:21
  110.6 0.0 all-reduce.3.cloned.1.call-start
  110.7 54.7 %all-to-all-done = bf16[256,8,256]{0,2,1:T(8,128)(2,1)} async-done(((bf16[256,8,256]{0,2,1:T(8,128)(2,1)}), bf16[256,8,256]{0,2,1:T(8,128)(2,1)}, u32[]{:S(2)}, u32[]{:S(2)}) %all-to-all-start) | async-done | bytes 1048608 | tf_op jit(solution)/shard_map/all_to_all | solution.py:21
  165.4 2.3 copy.14
  167.7 8.2 %fusion.55 = (f32[2048]{0:T(1024)}, f32[2048]{0:T(1024)}, f32[2048]{0:T(1024)}, f32[2048]{0:T(1024)}, f32[2048]{0:T(1024)}, /*index=5*/f32[2048]{0:T(1024)}, f32...) fusion(f32[286,2048]{1,0:T(8,128)S(1)} %maximum_convert_fusion,, ...), kind=kLoop, calls=%fused_computation.92 | loop fusion | flops 24080384 | bytes 42102784 | tf_op jit(solution)/shard_map/reduce_sum | solution.py:58
  175.9 0.7 slice.523
  176.6 1.5 collective-permute-start.1
  178.1 4.2 %fusion.54 = (f32[2048]{0:T(1024)}, f32[2048]{0:T(1024)}, f32[2048]{0:T(1024)}, f32[2048]{0:T(1024)}, f32[2048]{0:T(1024)}, /*index=5*/f32[2048]{0:T(1024)}, f32...) fusion(bf16[256,2048]{1,0:T(8,128)(2,1)S(1)} %get-tuple-element, ...), kind=kLoop, calls=%fused_computation.91 | loop fusion | flops 14129152 | bytes 28418048 | tf_op jit(solution)/shard_map/reduce_sum | solution.py:58
  182.3 6.1 %stack.131 = f32[32,2048]{1,0:T(8,128)} concatenate(f32[1,2048]{1,0:T(1,128)} %bitcast.178, f32[1,2048]{1,0:T(1,128)} %bitcast.180, f32[1,2048]{1,0:T(1,128)} %bitcast.181, f32[1,2048]{1,0:T(1,128)} %bitcast.182, f32[1,2048]{1,0:T(1,128)} %bitcast.183, f32[1,2048]{1,0:T(1,128)} %bitcast.184, f32[1,2048]{1,0:T(1,128)} %bitcast.185, f32[1,2048]{1,0:T(1,128)} %bitcast.186, ...), dimensions={0} | concatenate | bytes 524288 | tf_op jit(solution)/shard_map/stack | solution.py:59
  188.4 0.0 all-reduce.3.cloned.1.call-update
  188.5 0.0 all-reduce.5.cloned.1.call-start
  188.5 1.5 maximum_convert_fusion.1
  190.0 16.3 %all-gather.5.cloned.1.call-done = bf16[2048,2048]{1,0:T(8,128)(2,1)} async-done(((bf16[256,2048]{1,0:T(8,128)(2,1)}), bf16[2048,2048]{1,0:T(8,128)(2,1)}) %all-gather.5.cloned.1.call-update) | async-done | bytes 8388624 | tf_op jit(solution)/shard_map/all_gather | solution.py:39
  206.4 7.4 %convolution_bitcast_fusion = f32[256,2048]{0,1:T(8,128)} fusion(bf16[2048,2048]{1,0:T(8,128)(2,1)} %all-gather.5.cloned.1.call-done, bf16[2048,256]{1,0:T(8,128)(2,1)} %bitcast.103), kind=kOutput, calls=%fused_computation.31 | convolution fusion | flops 2147483648 | bytes 11534336 | tf_op jit(solution)/shard_map/dot_general | solution.py:68
  213.9 0.0 all-reduce.5.cloned.1.call-update
  213.9 0.5 copy-done.5
  214.5 0.0 copy-done.11
  214.5 0.0 copy-done.17
  214.6 0.0 copy-done.19
  214.6 0.0 copy-done.27
  214.6 0.0 copy-done.29
  214.7 0.0 copy-done.35
  214.7 10.6 %fusion.88 = (bf16[1,256,2048]{2,1,0:T(8,128)(2,1)}, bf16[256,2048]{1,0:T(8,128)(2,1)S(1)}) fusion(bf16[1,256,2048]{2,1,0:T(8,128)(2,1)} %param.6, bf16[1,256,2048]{2,1,0:T(8,128)(2,1)S(1)} %copy-done, f32[286,2048]{1,0:T(8,128)S(1)} %maximum_convert_fusion.1, f32[2048]{0:T(1024)S(1)} %bitcast.107, f32[2048]{0:T(1024)S(1)} %bitcast.109, ...), kind=kLoop, calls=%fused_computation.163 | loop fusion | flops 38273024 | bytes 69459968 | tf_op jit(solution)/shard_map/broadcast_in_dim | solution.py:72
  225.3 1.6 fusion.89
  226.8 110.4 %all-reduce.3.cloned.1.call-done = f32[32,2048]{1,0:T(8,128)} async-done(((f32[32,2048]{1,0:T(8,128)}), f32[32,2048]{1,0:T(8,128)}) %all-reduce.3.cloned.1.call-update) | async-done | bytes 262160 | tf_op jit(solution)/shard_map/psum | solution.py:59
  337.2 1.4 slice.556
  338.7 1.5 constant_dynamic-slice_fusion
  340.1 69.2 %all-reduce.5.cloned.1.call-done = f32[256,2048]{0,1:T(8,128)} async-done(((f32[256,2048]{0,1:T(8,128)}), f32[256,2048]{0,1:T(8,128)}) %all-reduce.5.cloned.1.call-update) | async-done | bytes 2097168 | tf_op jit(solution)/shard_map/psum | solution.py:71
  409.3 2.9 copy.15
  (99 shorter events, 0.3 us)
Async XLA Ops:
  7.2 2.3 copy-start
  7.2 87.2 %all-gather.3.cloned.1.call-start = ((), (), s32[]{:S(2)}) async-start(), calls=%async_computation.1 | async-start | bytes 9437184 | tf_op jit(solution)/shard_map/all_gather | solution.py:19
  7.9 198.4 %all-gather.5.cloned.1.call-start = ((), (), s32[]{:S(2)}) async-start(), calls=%async_computation.3 | async-start | bytes 9437184 | tf_op jit(solution)/shard_map/all_gather | solution.py:39
  9.4 5.3 %copy-start.49 = (f32[31,512]{1,0:T(8,128)S(1)}, f32[31,512]{1,0:T(8,128)}, u32[]{:S(2)}) copy-start(f32[31,512]{1,0:T(8,128)} %param.9) | copy-start | bytes 190468
  9.4 14.4 %copy-start.2 = (bf16[1,256,2048]{2,1,0:T(8,128)(2,1)S(1)}, bf16[1,256,2048]{2,1,0:T(8,128)(2,1)}, u32[]{:S(2)}) copy-start(bf16[1,256,2048]{2,1,0:T(8,128)(2,1)} %param.6) | copy-start | bytes 3145732
  9.8 15.0 %collective-permute-start = (bf16[30,2048]{1,0:T(8,128)(2,1)S(1)}, bf16[30,2048]{1,0:T(8,128)(2,1)S(1)}, u32[]{:S(2)}, u32[]{:S(2)}) collective-permute-start(bf16[30,2048]{1,0:T(8,128)(2,1)S(1)} %fusion.96), channel_id=1, source_target_pairs={{0,8},{8,16},{16,24},{1,9},{9,17},{17,25},{2,10},{10,18},{18,26},{... | collective-permute-start | bytes 368648 | tf_op jit(solution)/shard_map/ppermute | solution.py:24
  23.9 1.3 copy-start.4
  23.9 1.3 copy-start.6
  23.9 1.3 copy-start.8
  23.9 1.3 copy-start.10
  23.9 1.3 copy-start.12
  23.9 1.3 copy-start.14
  23.9 1.3 copy-start.16
  24.0 1.3 copy-start.18
  24.0 1.3 copy-start.20
  24.0 1.3 copy-start.22
  24.0 1.3 copy-start.24
  24.0 1.3 copy-start.26
  24.0 1.3 copy-start.28
  24.0 1.3 copy-start.30
  24.0 1.3 copy-start.32
  24.0 1.3 copy-start.34
  24.0 1.3 copy-start.36
  24.7 11.3 %copy-start.37 = (f32[1,2048]{1,0:T(1,128)}, f32[1,2048]{1,0:T(1,128)S(1)}, u32[]{:S(2)}) copy-start(f32[1,2048]{1,0:T(1,128)S(1)} %get-tuple-element.79) | copy-start | bytes 24580
  24.7 11.3 %copy-start.38 = (f32[1,2048]{1,0:T(1,128)}, f32[1,2048]{1,0:T(1,128)S(1)}, u32[]{:S(2)}) copy-start(f32[1,2048]{1,0:T(1,128)S(1)} %get-tuple-element.80) | copy-start | bytes 24580
  24.7 11.3 %copy-start.39 = (f32[1,2048]{1,0:T(1,128)}, f32[1,2048]{1,0:T(1,128)S(1)}, u32[]{:S(2)}) copy-start(f32[1,2048]{1,0:T(1,128)S(1)} %get-tuple-element.81) | copy-start | bytes 24580
  24.7 11.3 %copy-start.40 = (f32[1,2048]{1,0:T(1,128)}, f32[1,2048]{1,0:T(1,128)S(1)}, u32[]{:S(2)}) copy-start(f32[1,2048]{1,0:T(1,128)S(1)} %get-tuple-element.82) | copy-start | bytes 24580
  24.7 11.3 %copy-start.41 = (f32[1,2048]{1,0:T(1,128)}, f32[1,2048]{1,0:T(1,128)S(1)}, u32[]{:S(2)}) copy-start(f32[1,2048]{1,0:T(1,128)S(1)} %get-tuple-element.83) | copy-start | bytes 24580
  24.8 11.3 %copy-start.42 = (f32[1,2048]{1,0:T(1,128)}, f32[1,2048]{1,0:T(1,128)S(1)}, u32[]{:S(2)}) copy-start(f32[1,2048]{1,0:T(1,128)S(1)} %get-tuple-element.84) | copy-start | bytes 24580
  24.8 11.3 %copy-start.43 = (f32[1,2048]{1,0:T(1,128)}, f32[1,2048]{1,0:T(1,128)S(1)}, u32[]{:S(2)}) copy-start(f32[1,2048]{1,0:T(1,128)S(1)} %get-tuple-element.85) | copy-start | bytes 24580
  24.8 11.3 %copy-start.44 = (f32[1,2048]{1,0:T(1,128)}, f32[1,2048]{1,0:T(1,128)S(1)}, u32[]{:S(2)}) copy-start(f32[1,2048]{1,0:T(1,128)S(1)} %get-tuple-element.86) | copy-start | bytes 24580
  24.8 11.3 %copy-start.45 = (f32[1,2048]{1,0:T(1,128)}, f32[1,2048]{1,0:T(1,128)S(1)}, u32[]{:S(2)}) copy-start(f32[1,2048]{1,0:T(1,128)S(1)} %get-tuple-element.87) | copy-start | bytes 24580
  24.8 11.3 %copy-start.46 = (f32[1,2048]{1,0:T(1,128)}, f32[1,2048]{1,0:T(1,128)S(1)}, u32[]{:S(2)}) copy-start(f32[1,2048]{1,0:T(1,128)S(1)} %get-tuple-element.88) | copy-start | bytes 24580
  24.8 11.3 %copy-start.47 = (f32[1,2048]{1,0:T(1,128)}, f32[1,2048]{1,0:T(1,128)S(1)}, u32[]{:S(2)}) copy-start(f32[1,2048]{1,0:T(1,128)S(1)} %get-tuple-element.89) | copy-start | bytes 24580
  24.8 11.3 %copy-start.48 = (f32[1,2048]{1,0:T(1,128)}, f32[1,2048]{1,0:T(1,128)S(1)}, u32[]{:S(2)}) copy-start(f32[1,2048]{1,0:T(1,128)S(1)} %get-tuple-element.90) | copy-start | bytes 24580
  36.2 1.0 copy-start.3
  106.2 61.5 %copy-start.50 = (f32[2048]{0:T(1024)S(1)}, f32[2048]{0:T(1024)}, u32[]{:S(2)}) copy-start(f32[2048]{0:T(1024)} %param.10) | copy-start | bytes 24580
  106.2 59.1 %all-to-all-start = ((bf16[256,8,256]{0,2,1:T(8,128)(2,1)}), bf16[256,8,256]{0,2,1:T(8,128)(2,1)}, u32[]{:S(2)}, u32[]{:S(2)}) async-start(bf16[256,8,256]{0,2,1:T(8,128)(2,1)} %bitcast.102), calls=%async_computation | async-start | bytes 2097152 | tf_op jit(solution)/shard_map/all_to_all | solution.py:21
  110.6 226.6 %all-reduce.3.cloned.1.call-start = ((), (), s32[]{:S(2)}) async-start(), calls=%async_computation.2 | async-start | bytes 524288 | tf_op jit(solution)/shard_map/psum | solution.py:59
  175.9 6.4 %copy-start.1 = (bf16[256,2048]{1,0:T(8,128)(2,1)}, bf16[256,2048]{1,0:T(8,128)(2,1)S(1)}, u32[]{:S(2)}) copy-start(bf16[256,2048]{1,0:T(8,128)(2,1)S(1)} %get-tuple-element.54) | copy-start | bytes 3145732
  176.6 11.9 %collective-permute-start.1 = (bf16[30,2048]{1,0:T(8,128)(2,1)}, bf16[30,2048]{1,0:T(8,128)(2,1)S(1)}, u32[]{:S(2)}, u32[]{:S(2)}) collective-permute-start(bf16[30,2048]{1,0:T(8,128)(2,1)} %slice.523), channel_id=1, source_target_pairs={{8,0},{16,8},{24,16},{9,1},{17,9},{25,17},{10,2},{18,10},{26,18},{... | collective-permute-start | bytes 368648 | tf_op jit(solution)/shard_map/ppermute | solution.py:50
  188.5 220.8 %all-reduce.5.cloned.1.call-start = ((), (), s32[]{:S(2)}) async-start(), calls=%async_computation.4 | async-start | bytes 4194304 | tf_op jit(solution)/shard_map/psum | solution.py:71
  213.8 0.8 copy-start.25
  213.8 0.8 copy-start.27
  213.9 0.8 copy-start.29
  213.9 0.8 copy-start.31
  213.9 0.8 copy-start.33
  213.9 0.8 copy-start.35
  (10 other events, 7.5 us)
Sparse Core Ops, SparseCore 0:
  9.6 84.7 all-gather.2
  104.0 102.3 all-gather.4
  211.9 125.3 all-reduce.2
  340.8 68.5 all-reduce.4
where the time goes:
time: 419 us
  waiting for transfers between devices  308 us (74%)
  other arithmetic  39.9 us (10%)
  local copies, waits for them, and re-layouts  19.3 us (5%)
  matrix products  16.9 us (4%)
  between operations  14.5 us (3%)
  starting transfers between devices  10.9 us (3%)
  blocking collectives  9.08 us (2%)
    psum x1, waiting for transfers between devices, body(): sums = lax.psum(jnp.stack(terms + [gain_part]), ('sp', 'dp'))  110 us
    psum x1, waiting for transfers between devices, body(): grad_weight = lax.psum(owned, 'sp')  69.2 us
    all_gather x1, waiting for transfers between devices, body(): weight = lax.all_gather(out_weight, 'dp', axis=0, tiled=True)  56.8 us
    all_to_all x1, waiting for transfers between devices, body(): lax.all_to_all(up, 'dp', split_axis=1, concat_axis=0, tiled=True)  54.7 us
    all_gather x1, waiting for transfers between devices, body(): act_all = lax.all_gather(activated, 'dp', axis=0, tiled=True)  16.3 us
    reduce_sum x2, other arithmetic, body(): terms.append(jnp.sum(here * padded[j:j + length], axis=0))  12.5 us
    reduce_sum x1, other arithmetic, body(): mean = jnp.mean(conv, axis=-1, keepdims=True)  10.7 us
    broadcast_in_dim x1, other arithmetic, body(): grad_gate[None]  10.6 us
  transfers between devices with their start and end apart: 7, of which 5 were waited for; matrix products, arithmetic and copies ran while one was open for 15% of the time, Pallas kernels for 0%

commit v1 on v0

--- a/solution.py
+++ b/solution.py
@@ -68,7 +68,11 @@
     owned = lax.dot_general(
         up_columns, act_all, (((0,), (0,)), ((), ())), preferred_element_type=f32
     )
-    grad_weight = lax.psum(owned, "sp")
+    grad_weight = owned
+    for hop in (1, 2):
+        grad_weight = grad_weight + lax.ppermute(
+            grad_weight, "sp", [(dev, dev ^ hop) for dev in range(4)]
+        )
     return (grad_value[None], grad_gate[None], grad_taps, grad_gain, grad_weight)
 
 

time: 419 us -> 378 us (0.902)
  waiting for transfers between devices: 308 us -> 260 us
    psum x1 -> x0, waiting for transfers between devices: 69.2 us -> none  [body(): grad_weight = lax.psum(owned, 'sp')]
    psum x1, waiting for transfers between devices: 110 us -> 79.1 us  [body(): sums = lax.psum(jnp.stack(terms + [gain_part]), ('sp', 'dp'))]
    ppermute x1, waiting for transfers between devices: 0.01 us -> 30.4 us  [body(): after = lax.ppermute(grad_conv[:halo], 'sp', back)]
    all_gather x1, waiting for transfers between devices: 16.3 us -> 38.7 us  [body(): act_all = lax.all_gather(activated, 'dp', axis=0, tiled=True)]
    add x0 -> x2, other arithmetic: none -> 5.88 us  [body(): grad_weight + lax.ppermute(grad_weight, 'sp', [(dev, dev ^ hop) for dev i...]
  transfers between devices with their start and end apart: 7 -> 8, of which waited for: 5 -> 5; matrix products, arithmetic and copies ran while one was open for 15% -> 15% of each run, Pallas kernels for 0% -> 0%
where the time goes in v1:
time: 378 us; the launch traced here: 377 us
  waiting for transfers between devices  260 us (69%)
  other arithmetic  43.6 us (12%)
  local copies, waits for them, and re-layouts  18.6 us (5%)
  matrix products  17.1 us (5%)
  between operations  14.8 us (4%)
  starting transfers between devices  13.7 us (4%)
  blocking collectives  9.08 us (2%)
    psum x1, waiting for transfers between devices, body(): sums = lax.psum(jnp.stack(terms + [gain_part]), ('sp', 'dp'))  79.1 us
    all_gather x1, waiting for transfers between devices, body(): weight = lax.all_gather(out_weight, 'dp', axis=0, tiled=True)  56.8 us
    all_to_all x1, waiting for transfers between devices, body(): lax.all_to_all(up, 'dp', split_axis=1, concat_axis=0, tiled=True)  54.5 us
    all_gather x1, waiting for transfers between devices, body(): act_all = lax.all_gather(activated, 'dp', axis=0, tiled=True)  38.7 us
    ppermute x1, waiting for transfers between devices, body(): after = lax.ppermute(grad_conv[:halo], 'sp', back)  30.4 us
    reduce_sum x2, other arithmetic, body(): terms.append(jnp.sum(here * padded[j:j + length], axis=0))  11.3 us
    reduce_sum x1, other arithmetic, body(): mean = jnp.mean(conv, axis=-1, keepdims=True)  10.7 us
    broadcast_in_dim x1, other arithmetic, body(): grad_gate[None]  9.5 us
  transfers between devices with their start and end apart: 8, of which 5 were waited for; matrix products, arithmetic and copies ran while one was open for 15% of the time, Pallas kernels for 0%

profile of v1, /device:TPU:0, one launch (start us, length us, event | category | flops | bytes accessed | tf_op | source)
XLA Modules:
  0.0 377.1 jit_solution(6353236624788869922)
XLA Ops:
  7.2 0.0 copy-start.2
  7.2 0.0 all-gather.3.cloned.1.call-start
  7.2 0.7 all-gather.3.cloned.1.call-update
  7.9 0.0 all-gather.5.cloned.1.call-start
  8.0 1.5 convert_element_type.50
  9.4 0.0 copy-start.65
  9.4 0.0 copy-start
  9.5 0.2 convert_element_type.49
  9.7 0.1 fusion.96
  9.8 4.9 %collective-permute-start = (bf16[30,2048]{1,0:T(8,128)(2,1)S(1)}, bf16[30,2048]{1,0:T(8,128)(2,1)S(1)}, u32[]{:S(2)}, u32[]{:S(2)}) collective-permute-start(bf16[30,2048]{1,0:T(8,128)(2,1)S(1)} %fusion.96), channel_id=1, source_target_pairs={{0,8},{8,16},{16,24},{1,9},{9,17},{17,25},{2,10},{10,18},{18,26},{... | collective-permute-start | bytes 368648 | tf_op jit(solution)/shard_map/ppermute | solution.py:24
  14.7 9.1 %all_gather.9 = f32[31,2048]{1,0:T(8,128)S(1)} all-gather(f32[31,512]{1,0:T(8,128)S(1)} %copy-done.65), channel_id=1, replica_groups=mesh['sp'=4,'dp'=8] {'sp'}, dimensions={1}, use_global_device_ids=true | all-gather | bytes 317440 | tf_op jit(solution)/shard_map/all_gather | solution.py:22
  23.8 0.1 fusion.99
  24.1 0.6 fusion.87
  24.6 0.1 fusion.100
  24.8 0.3 maximum_convert_fusion
  25.3 10.7 %convert_reduce_fusion = (f32[256]{0:T(256)S(1)}, bf16[256,2048]{1,0:T(8,128)(2,1)S(1)}) fusion(f32[286,2048]{1,0:T(8,128)S(1)} %maximum_convert_fusion, f32[2048]{0:T(1024)S(1)} %bitcast.106, f32[2048]{0:T(1024)S(1)} %bitcast.108, f32[2048]{0:T(1024)S(1)} %bitcast.110, f32[2048]{0:T(1024)S(1)} %bitcast.112, f32[2048]{0:T(1024)S(1)} %bitcast.114, ...), kind=kLoop, calls=%fused_computation.37 | loop fusion | flops 33554176 | bytes 66315264 | tf_op jit(solution)/shard_map/reduce_sum | solution.py:32
  36.2 0.0 copy-start.4
  36.2 0.9 copy-done.4
  37.1 0.4 fusion.20
  37.6 56.8 %all-gather.3.cloned.1.call-done = bf16[2048,2048]{1,0:T(8,128)(2,1)} async-done(((bf16[256,2048]{1,0:T(8,128)(2,1)}), bf16[2048,2048]{1,0:T(8,128)(2,1)}) %all-gather.3.cloned.1.call-update) | async-done | bytes 8388624 | tf_op jit(solution)/shard_map/all_gather | solution.py:19
  94.4 9.5 %fusion.19 = (f32[2048]{0:T(1024)}, f32[256]{0:T(256)S(1)}, f32[256]{0:T(256)S(1)}, bf16[256,2048]{1,0:T(8,128)(2,1)}, f32[256,2048]{1,0:T(8,128)}) fusion(bf16[256,2048]{1,0:T(8,128)(2,1)} %copy-done.4, f32[256]{0:T(256)S(1)} %add_rsqrt_fusion, f32[256]{0:T(256)S(1)} %broadcast_multiply_fusion.2, f32[2048]{0:T(1024)} %param.10, ...), kind=kOutput, calls=%fused_computation.56 | convolution fusion | flops 2157966848 | bytes 13651968 | tf_op jit(solution)/shard_map/dot_general | solution.py:40
  103.9 0.0 all-gather.5.cloned.1.call-update
  103.9 2.3 copy.13
  106.1 4.3 %all-to-all-start = ((bf16[256,8,256]{0,2,1:T(8,128)(2,1)}), bf16[256,8,256]{0,2,1:T(8,128)(2,1)}, u32[]{:S(2)}, u32[]{:S(2)}) async-start(bf16[256,8,256]{0,2,1:T(8,128)(2,1)} %bitcast.102), calls=%async_computation | async-start | bytes 2097152 | tf_op jit(solution)/shard_map/all_to_all | solution.py:21
  110.4 0.2 all-reduce.2.cloned.1.call-start
  110.6 54.5 %all-to-all-done = bf16[256,8,256]{0,2,1:T(8,128)(2,1)} async-done(((bf16[256,8,256]{0,2,1:T(8,128)(2,1)}), bf16[256,8,256]{0,2,1:T(8,128)(2,1)}, u32[]{:S(2)}, u32[]{:S(2)}) %all-to-all-start) | async-done | bytes 1048608 | tf_op jit(solution)/shard_map/all_to_all | solution.py:21
  165.2 2.3 copy.14
  167.4 38.7 %all-gather.5.cloned.1.call-done = bf16[2048,2048]{1,0:T(8,128)(2,1)} async-done(((bf16[256,2048]{1,0:T(8,128)(2,1)}), bf16[2048,2048]{1,0:T(8,128)(2,1)}) %all-gather.5.cloned.1.call-update) | async-done | bytes 8388624 | tf_op jit(solution)/shard_map/all_gather | solution.py:39
  206.2 7.6 %convolution_bitcast_fusion = f32[256,2048]{0,1:T(8,128)} fusion(bf16[2048,2048]{1,0:T(8,128)(2,1)} %all-gather.5.cloned.1.call-done, bf16[2048,256]{1,0:T(8,128)(2,1)} %bitcast.103), kind=kOutput, calls=%fused_computation.31 | convolution fusion | flops 2147483648 | bytes 11534336 | tf_op jit(solution)/shard_map/dot_general | solution.py:68
  213.8 1.5 collective-permute-start.2
  215.3 7.1 %fusion.55 = (f32[2048]{0:T(1024)}, f32[2048]{0:T(1024)}, f32[2048]{0:T(1024)}, f32[2048]{0:T(1024)}, f32[2048]{0:T(1024)}, /*index=5*/f32[2048]{0:T(1024)}, f32...) fusion(f32[286,2048]{1,0:T(8,128)S(1)} %maximum_convert_fusion,, ...), kind=kLoop, calls=%fused_computation.92 | loop fusion | flops 24080384 | bytes 42102784 | tf_op jit(solution)/shard_map/reduce_sum | solution.py:58
  222.4 0.7 slice.523
  223.1 1.3 collective-permute-start.1
  224.4 4.2 %fusion.54 = (f32[2048]{0:T(1024)}, f32[2048]{0:T(1024)}, f32[2048]{0:T(1024)}, f32[2048]{0:T(1024)}, f32[2048]{0:T(1024)}, /*index=5*/f32[2048]{0:T(1024)}, f32...) fusion(bf16[256,2048]{1,0:T(8,128)(2,1)S(1)} %get-tuple-element, ...), kind=kLoop, calls=%fused_computation.91 | loop fusion | flops 14129152 | bytes 28418048 | tf_op jit(solution)/shard_map/reduce_sum | solution.py:58
  228.6 6.1 %stack.131 = f32[32,2048]{1,0:T(8,128)} concatenate(f32[1,2048]{1,0:T(1,128)} %bitcast.178, f32[1,2048]{1,0:T(1,128)} %bitcast.180, f32[1,2048]{1,0:T(1,128)} %bitcast.181, f32[1,2048]{1,0:T(1,128)} %bitcast.182, f32[1,2048]{1,0:T(1,128)} %bitcast.183, f32[1,2048]{1,0:T(1,128)} %bitcast.184, f32[1,2048]{1,0:T(1,128)} %bitcast.185, f32[1,2048]{1,0:T(1,128)} %bitcast.186, ...), dimensions={0} | concatenate | bytes 524288 | tf_op jit(solution)/shard_map/stack | solution.py:59
  234.8 0.0 all-reduce.2.cloned.1.call-update
  234.8 30.4 %collective-permute-done.1 = bf16[30,2048]{1,0:T(8,128)(2,1)S(1)} collective-permute-done((bf16[30,2048]{1,0:T(8,128)(2,1)}, bf16[30,2048]{1,0:T(8,128)(2,1)S(1)}, u32[]{:S(2)}, u32[]{:S(2)}) %collective-permute-start.1) | collective-permute-done | bytes 122912 | tf_op jit(solution)/shard_map/ppermute | solution.py:50
  265.1 1.5 maximum_convert_fusion.1
  266.6 0.0 copy-start.3
  266.9 2.7 add.289
  269.7 1.5 collective-permute-start.3
  271.5 9.5 %fusion.88 = (bf16[1,256,2048]{2,1,0:T(8,128)(2,1)}, bf16[256,2048]{1,0:T(8,128)(2,1)S(1)}) fusion(bf16[1,256,2048]{2,1,0:T(8,128)(2,1)S(1)} %copy-done.3, bf16[1,256,2048]{2,1,0:T(8,128)(2,1)S(1)} %copy-done, f32[286,2048]{1,0:T(8,128)S(1)} %maximum_convert_fusion.1, f32[2048]{0:T(1024)S(1)} %bitcast.107, f32[2048]{0:T(1024)S(1)} %bitcast.109, ...), kind=kLoop, calls=%fused_computation.163 | loop fusion | flops 38273024 | bytes 69459968 | tf_op jit(solution)/shard_map/broadcast_in_dim | solution.py:76
  281.0 1.6 fusion.89
  282.5 79.1 %all-reduce.2.cloned.1.call-done = f32[32,2048]{1,0:T(8,128)} async-done(((f32[32,2048]{1,0:T(8,128)}), f32[32,2048]{1,0:T(8,128)}) %all-reduce.2.cloned.1.call-update) | async-done | bytes 262160 | tf_op jit(solution)/shard_map/psum | solution.py:59
  361.6 1.4 slice.556
  363.0 1.5 constant_dynamic-slice_fusion
  364.5 3.2 add.290
  367.6 2.9 copy.15
  (134 shorter events, 0.3 us)
Async XLA Ops:
  7.2 87.2 %all-gather.3.cloned.1.call-start = ((), (), s32[]{:S(2)}) async-start(), calls=%async_computation.1 | async-start | bytes 9437184 | tf_op jit(solution)/shard_map/all_gather | solution.py:19
  7.9 198.3 %all-gather.5.cloned.1.call-start = ((), (), s32[]{:S(2)}) async-start(), calls=%async_computation.3 | async-start | bytes 9437184 | tf_op jit(solution)/shard_map/all_gather | solution.py:39
  9.4 5.3 %copy-start.65 = (f32[31,512]{1,0:T(8,128)S(1)}, f32[31,512]{1,0:T(8,128)}, u32[]{:S(2)}) copy-start(f32[31,512]{1,0:T(8,128)} %param.9) | copy-start | bytes 190468
  9.4 14.4 %copy-start = (bf16[1,256,2048]{2,1,0:T(8,128)(2,1)S(1)}, bf16[1,256,2048]{2,1,0:T(8,128)(2,1)}, u32[]{:S(2)}) copy-start(bf16[1,256,2048]{2,1,0:T(8,128)(2,1)} %param.7) | copy-start | bytes 3145732
  9.8 15.0 %collective-permute-start = (bf16[30,2048]{1,0:T(8,128)(2,1)S(1)}, bf16[30,2048]{1,0:T(8,128)(2,1)S(1)}, u32[]{:S(2)}, u32[]{:S(2)}) collective-permute-start(bf16[30,2048]{1,0:T(8,128)(2,1)S(1)} %fusion.96), channel_id=1, source_target_pairs={{0,8},{8,16},{16,24},{1,9},{9,17},{17,25},{2,10},{10,18},{18,26},{... | collective-permute-start | bytes 368648 | tf_op jit(solution)/shard_map/ppermute | solution.py:24
  24.7 11.3 %copy-start.41 = (f32[1,2048]{1,0:T(1,128)}, f32[1,2048]{1,0:T(1,128)S(1)}, u32[]{:S(2)}) copy-start(f32[1,2048]{1,0:T(1,128)S(1)} %get-tuple-element.79) | copy-start | bytes 24580
  24.7 11.3 %copy-start.43 = (f32[1,2048]{1,0:T(1,128)}, f32[1,2048]{1,0:T(1,128)S(1)}, u32[]{:S(2)}) copy-start(f32[1,2048]{1,0:T(1,128)S(1)} %get-tuple-element.80) | copy-start | bytes 24580
  24.7 11.3 %copy-start.45 = (f32[1,2048]{1,0:T(1,128)}, f32[1,2048]{1,0:T(1,128)S(1)}, u32[]{:S(2)}) copy-start(f32[1,2048]{1,0:T(1,128)S(1)} %get-tuple-element.81) | copy-start | bytes 24580
  24.7 11.3 %copy-start.47 = (f32[1,2048]{1,0:T(1,128)}, f32[1,2048]{1,0:T(1,128)S(1)}, u32[]{:S(2)}) copy-start(f32[1,2048]{1,0:T(1,128)S(1)} %get-tuple-element.82) | copy-start | bytes 24580
  24.8 11.3 %copy-start.49 = (f32[1,2048]{1,0:T(1,128)}, f32[1,2048]{1,0:T(1,128)S(1)}, u32[]{:S(2)}) copy-start(f32[1,2048]{1,0:T(1,128)S(1)} %get-tuple-element.83) | copy-start | bytes 24580
  24.8 11.3 %copy-start.51 = (f32[1,2048]{1,0:T(1,128)}, f32[1,2048]{1,0:T(1,128)S(1)}, u32[]{:S(2)}) copy-start(f32[1,2048]{1,0:T(1,128)S(1)} %get-tuple-element.84) | copy-start | bytes 24580
  24.8 11.3 %copy-start.53 = (f32[1,2048]{1,0:T(1,128)}, f32[1,2048]{1,0:T(1,128)S(1)}, u32[]{:S(2)}) copy-start(f32[1,2048]{1,0:T(1,128)S(1)} %get-tuple-element.85) | copy-start | bytes 24580
  24.8 11.3 %copy-start.55 = (f32[1,2048]{1,0:T(1,128)}, f32[1,2048]{1,0:T(1,128)S(1)}, u32[]{:S(2)}) copy-start(f32[1,2048]{1,0:T(1,128)S(1)} %get-tuple-element.86) | copy-start | bytes 24580
  24.8 11.3 %copy-start.57 = (f32[1,2048]{1,0:T(1,128)}, f32[1,2048]{1,0:T(1,128)S(1)}, u32[]{:S(2)}) copy-start(f32[1,2048]{1,0:T(1,128)S(1)} %get-tuple-element.87) | copy-start | bytes 24580
  24.8 11.3 %copy-start.59 = (f32[1,2048]{1,0:T(1,128)}, f32[1,2048]{1,0:T(1,128)S(1)}, u32[]{:S(2)}) copy-start(f32[1,2048]{1,0:T(1,128)S(1)} %get-tuple-element.88) | copy-start | bytes 24580
  24.8 11.3 %copy-start.61 = (f32[1,2048]{1,0:T(1,128)}, f32[1,2048]{1,0:T(1,128)S(1)}, u32[]{:S(2)}) copy-start(f32[1,2048]{1,0:T(1,128)S(1)} %get-tuple-element.89) | copy-start | bytes 24580
  24.8 11.3 %copy-start.63 = (f32[1,2048]{1,0:T(1,128)}, f32[1,2048]{1,0:T(1,128)S(1)}, u32[]{:S(2)}) copy-start(f32[1,2048]{1,0:T(1,128)S(1)} %get-tuple-element.90) | copy-start | bytes 24580
  106.1 59.0 %all-to-all-start = ((bf16[256,8,256]{0,2,1:T(8,128)(2,1)}), bf16[256,8,256]{0,2,1:T(8,128)(2,1)}, u32[]{:S(2)}, u32[]{:S(2)}) async-start(bf16[256,8,256]{0,2,1:T(8,128)(2,1)} %bitcast.102), calls=%async_computation | async-start | bytes 2097152 | tf_op jit(solution)/shard_map/all_to_all | solution.py:21
  110.4 251.2 %all-reduce.2.cloned.1.call-start = ((), (), s32[]{:S(2)}) async-start(), calls=%async_computation.2 | async-start | bytes 524288 | tf_op jit(solution)/shard_map/psum | solution.py:59
  206.2 9.1 %copy-start.5 = (bf16[256,2048]{1,0:T(8,128)(2,1)S(1)}, bf16[256,2048]{1,0:T(8,128)(2,1)}, u32[]{:S(2)}) copy-start(bf16[256,2048]{1,0:T(8,128)(2,1)} %copy-done.4) | copy-start | bytes 3145732
  206.2 9.1 %copy-start.6 = (f32[256,2048]{1,0:T(8,128)S(1)}, f32[256,2048]{1,0:T(8,128)}, u32[]{:S(2)}) copy-start(f32[256,2048]{1,0:T(8,128)} %get-tuple-element.91) | copy-start | bytes 6291460
  206.2 9.1 %copy-start.66 = (f32[2048]{0:T(1024)S(1)}, f32[2048]{0:T(1024)}, u32[]{:S(2)}) copy-start(f32[2048]{0:T(1024)} %param.10) | copy-start | bytes 24580
  213.8 53.1 %collective-permute-start.2 = (f32[256,2048]{0,1:T(8,128)}, f32[256,2048]{0,1:T(8,128)}, u32[]{:S(2)}, u32[]{:S(2)}) collective-permute-start(f32[256,2048]{0,1:T(8,128)} %convolution_bitcast_fusion), channel_id=1, source_target_pairs={{0,8},{8,0},{16,24},{24,16},{1,9},{9,1},{17,25},{25,17},{2,10},{10... | collective-permute-start | bytes 6291464 | tf_op jit(solution)/shard_map/ppermute | solution.py:73
  222.4 6.2 %copy-start.1 = (bf16[256,2048]{1,0:T(8,128)(2,1)}, bf16[256,2048]{1,0:T(8,128)(2,1)S(1)}, u32[]{:S(2)}) copy-start(bf16[256,2048]{1,0:T(8,128)(2,1)S(1)} %get-tuple-element.54) | copy-start | bytes 3145732
  223.1 42.0 %collective-permute-start.1 = (bf16[30,2048]{1,0:T(8,128)(2,1)}, bf16[30,2048]{1,0:T(8,128)(2,1)S(1)}, u32[]{:S(2)}, u32[]{:S(2)}) collective-permute-start(bf16[30,2048]{1,0:T(8,128)(2,1)} %slice.523), channel_id=1, source_target_pairs={{8,0},{16,8},{24,16},{9,1},{17,9},{25,17},{10,2},{18,10},{26,18},{... | collective-permute-start | bytes 368648 | tf_op jit(solution)/shard_map/ppermute | solution.py:50
  266.6 4.6 %copy-start.3 = (bf16[1,256,2048]{2,1,0:T(8,128)(2,1)S(1)}, bf16[1,256,2048]{2,1,0:T(8,128)(2,1)}, u32[]{:S(2)}) copy-start(bf16[1,256,2048]{2,1,0:T(8,128)(2,1)} %param.6) | copy-start | bytes 3145732
  266.6 4.6 %copy-start.8 = (f32[1,2048]{1,0:T(1,128)S(1)}, f32[1,2048]{1,0:T(1,128)}, u32[]{:S(2)}) copy-start(f32[1,2048]{1,0:T(1,128)} %copy-done.7) | copy-start | bytes 24580
  266.6 4.5 %copy-start.10 = (f32[1,2048]{1,0:T(1,128)S(1)}, f32[1,2048]{1,0:T(1,128)}, u32[]{:S(2)}) copy-start(f32[1,2048]{1,0:T(1,128)} %copy-done.9) | copy-start | bytes 24580
  266.7 4.5 %copy-start.12 = (f32[1,2048]{1,0:T(1,128)S(1)}, f32[1,2048]{1,0:T(1,128)}, u32[]{:S(2)}) copy-start(f32[1,2048]{1,0:T(1,128)} %copy-done.11) | copy-start | bytes 24580
  266.7 4.5 %copy-start.14 = (f32[1,2048]{1,0:T(1,128)S(1)}, f32[1,2048]{1,0:T(1,128)}, u32[]{:S(2)}) copy-start(f32[1,2048]{1,0:T(1,128)} %copy-done.13) | copy-start | bytes 24580
  266.7 4.5 %copy-start.16 = (f32[1,2048]{1,0:T(1,128)S(1)}, f32[1,2048]{1,0:T(1,128)}, u32[]{:S(2)}) copy-start(f32[1,2048]{1,0:T(1,128)} %copy-done.15) | copy-start | bytes 24580
  266.7 4.5 %copy-start.18 = (f32[1,2048]{1,0:T(1,128)S(1)}, f32[1,2048]{1,0:T(1,128)}, u32[]{:S(2)}) copy-start(f32[1,2048]{1,0:T(1,128)} %copy-done.17) | copy-start | bytes 24580
  266.7 4.5 %copy-start.20 = (f32[1,2048]{1,0:T(1,128)S(1)}, f32[1,2048]{1,0:T(1,128)}, u32[]{:S(2)}) copy-start(f32[1,2048]{1,0:T(1,128)} %copy-done.19) | copy-start | bytes 24580
  266.7 4.5 %copy-start.22 = (f32[1,2048]{1,0:T(1,128)S(1)}, f32[1,2048]{1,0:T(1,128)}, u32[]{:S(2)}) copy-start(f32[1,2048]{1,0:T(1,128)} %copy-done.21) | copy-start | bytes 24580
  266.7 4.5 %copy-start.24 = (f32[1,2048]{1,0:T(1,128)S(1)}, f32[1,2048]{1,0:T(1,128)}, u32[]{:S(2)}) copy-start(f32[1,2048]{1,0:T(1,128)} %copy-done.23) | copy-start | bytes 24580
  266.7 4.5 %copy-start.26 = (f32[1,2048]{1,0:T(1,128)S(1)}, f32[1,2048]{1,0:T(1,128)}, u32[]{:S(2)}) copy-start(f32[1,2048]{1,0:T(1,128)} %copy-done.25) | copy-start | bytes 24580
  266.7 4.5 %copy-start.28 = (f32[1,2048]{1,0:T(1,128)S(1)}, f32[1,2048]{1,0:T(1,128)}, u32[]{:S(2)}) copy-start(f32[1,2048]{1,0:T(1,128)} %copy-done.27) | copy-start | bytes 24580
  266.7 4.5 %copy-start.30 = (f32[1,2048]{1,0:T(1,128)S(1)}, f32[1,2048]{1,0:T(1,128)}, u32[]{:S(2)}) copy-start(f32[1,2048]{1,0:T(1,128)} %copy-done.29) | copy-start | bytes 24580
  266.8 4.5 %copy-start.32 = (f32[1,2048]{1,0:T(1,128)S(1)}, f32[1,2048]{1,0:T(1,128)}, u32[]{:S(2)}) copy-start(f32[1,2048]{1,0:T(1,128)} %copy-done.31) | copy-start | bytes 24580
  266.8 4.5 %copy-start.34 = (f32[1,2048]{1,0:T(1,128)S(1)}, f32[1,2048]{1,0:T(1,128)}, u32[]{:S(2)}) copy-start(f32[1,2048]{1,0:T(1,128)} %copy-done.33) | copy-start | bytes 24580
  266.8 4.5 %copy-start.36 = (f32[1,2048]{1,0:T(1,128)S(1)}, f32[1,2048]{1,0:T(1,128)}, u32[]{:S(2)}) copy-start(f32[1,2048]{1,0:T(1,128)} %copy-done.35) | copy-start | bytes 24580
  266.8 4.5 %copy-start.38 = (f32[1,2048]{1,0:T(1,128)S(1)}, f32[1,2048]{1,0:T(1,128)}, u32[]{:S(2)}) copy-start(f32[1,2048]{1,0:T(1,128)} %copy-done.37) | copy-start | bytes 24580
  266.8 4.5 %copy-start.40 = (f32[1,2048]{1,0:T(1,128)S(1)}, f32[1,2048]{1,0:T(1,128)}, u32[]{:S(2)}) copy-start(f32[1,2048]{1,0:T(1,128)} %copy-done.39) | copy-start | bytes 24580
  266.8 4.5 %copy-start.42 = (f32[1,2048]{1,0:T(1,128)S(1)}, f32[1,2048]{1,0:T(1,128)}, u32[]{:S(2)}) copy-start(f32[1,2048]{1,0:T(1,128)} %copy-done.41) | copy-start | bytes 24580
  266.8 4.5 %copy-start.44 = (f32[1,2048]{1,0:T(1,128)S(1)}, f32[1,2048]{1,0:T(1,128)}, u32[]{:S(2)}) copy-start(f32[1,2048]{1,0:T(1,128)} %copy-done.43) | copy-start | bytes 24580
  266.8 4.5 %copy-start.46 = (f32[1,2048]{1,0:T(1,128)S(1)}, f32[1,2048]{1,0:T(1,128)}, u32[]{:S(2)}) copy-start(f32[1,2048]{1,0:T(1,128)} %copy-done.45) | copy-start | bytes 24580
  266.8 4.5 %copy-start.48 = (f32[1,2048]{1,0:T(1,128)S(1)}, f32[1,2048]{1,0:T(1,128)}, u32[]{:S(2)}) copy-start(f32[1,2048]{1,0:T(1,128)} %copy-done.47) | copy-start | bytes 24580
  269.7 94.8 %collective-permute-start.3 = (f32[256,2048]{0,1:T(8,128)S(1)}, f32[256,2048]{0,1:T(8,128)}, u32[]{:S(2)}, u32[]{:S(2)}) collective-permute-start(f32[256,2048]{0,1:T(8,128)S(1)} %add.289), channel_id=1, source_target_pairs={{0,16},{8,24},{16,0},{24,8},{1,17},{9,25},{17,1},{25,9},{2,18},{10... | collective-permute-start | bytes 6291464 | tf_op jit(solution)/shard_map/ppermute | solution.py:73
  (27 other events, 61.0 us)
Sparse Core Ops, SparseCore 0:
  9.6 84.7 all-gather.2
  104.0 102.1 all-gather.4
  234.9 126.6 all-reduce.1
